TPU v7x, 32 devices: a whole 2x2x4 slice. The times are simulated.
32 devices in a mesh: ep: 8 (over z, core), tp: 4 (over y, x).
Axes of the slice: x: 2, y: 2, z: 4, core: 2. Of those that a mesh axis runs over, the one named last changes fastest.
Arguments:
- tokens: bfloat16 [2048, 2048], P('ep'), may hold values from -6 to 6
- norm_gain: float32 [2048], replicated, may hold values from 0.1 to 1.9
- route_ids: int32 [2048, 4], P('ep'), may hold values from 0 to 15, all different within a row; in each aligned block of 256 rows (0 to 255, 256 to 511, ...) at most 96 rows name the same one
- route_weights: float32 [2048, 4], P('ep'), may hold values from 0.1 to 1
- w_gate: bfloat16 [16, 2048, 2048], P('ep', None, 'tp'), may hold values from -0.33007812 to 0.33007812
- w_up: bfloat16 [16, 2048, 2048], P('ep', None, 'tp'), may hold values from -0.33007812 to 0.33007812
- w_down: bfloat16 [16, 2048, 2048], P('ep', None, 'tp'), may hold values from -0.026489258 to 0.026489258
Outputs:
- mixed_out: bfloat16 [2048, 2048], P('ep', 'tp')
Inputs may be any that keep to these rules, and one draw needn't show every extreme that they name: `route_ids`: each token names 4 different experts. Within the tokens of one index of ep (aligned blocks of 256 tokens) no expert is named more than 96 times, a bound that some block reaches.
All inputs are finite; a program needn't handle non-finite values.
Results may differ from a plain program's by a relative error of at most 0.007.
Values may be sent and summed in bfloat16 or wider, within the bound.
A program may use at most 64 MiB of HBM per device.

v0:
```python
import jax
import jax.numpy as jnp
from jax import lax
from jax.sharding import PartitionSpec as P

swiglu_limit = 7.0
swiglu_alpha = 1.702
norm_eps = 1e-05


def clamped_units(gate_pre, up_pre):
    capped = jnp.minimum(gate_pre, swiglu_limit)
    linear = jnp.clip(up_pre, -swiglu_limit, swiglu_limit)
    return capped * jax.nn.sigmoid(swiglu_alpha * capped) * (linear + 1.0)


def expert_work(outgoing, gate_weight, up_weight, down_weight):
    received = lax.all_to_all(outgoing, "ep", split_axis=1, concat_axis=1, tiled=True)
    local_count, sources, capacity, columns = received.shape
    row_count = sources * capacity
    row_block = received.reshape(local_count, row_count, columns)
    shard_piece = lax.all_gather(row_block, "tp", axis=2, tiled=True)
    gate_sum = jnp.einsum(
        "lrd,ldf->lrf", shard_piece, gate_weight, preferred_element_type=jnp.float32
    )
    up_sum = jnp.einsum("lrd,ldf->lrf", shard_piece, up_weight, preferred_element_type=jnp.float32)
    activation = clamped_units(gate_sum, up_sum).astype(jnp.bfloat16)
    out_cols = down_weight.shape[2]
    result = jnp.einsum(
        "lrf,lfd->lrd",
        lax.all_gather(activation, "tp", axis=2, tiled=True),
        down_weight,
        preferred_element_type=jnp.float32,
    )
    result = result.astype(jnp.bfloat16).reshape(local_count, sources, capacity, out_cols)
    return lax.all_to_all(result, "ep", split_axis=1, concat_axis=1, tiled=True)


def per_device(tokens, norm_gain, route_ids, route_weights, w_gate, w_up, w_down):
    local_count = w_gate.shape[0]
    sources = lax.axis_size("ep")
    tp_count = lax.axis_size("tp")
    width = tokens.shape[1]
    columns = width // tp_count
    experts = local_count * sources
    tok_rows, top_count = route_ids.shape
    capacity = 3 * tok_rows * top_count // (2 * experts)
    values = tokens.astype(jnp.float32)
    row_mean = jnp.mean(values, axis=1, keepdims=True)
    centred = values - row_mean
    row_var = jnp.mean(centred * centred, axis=1, keepdims=True)
    offset = lax.axis_index("tp") * columns
    own_cols = lax.dynamic_slice_in_dim(centred, offset, columns, 1)
    own_gain = lax.dynamic_slice_in_dim(norm_gain, offset, columns, 0)
    normed = (own_cols * lax.rsqrt(row_var + norm_eps) * own_gain).astype(jnp.bfloat16)
    flat_ids = route_ids.reshape(-1)
    matches = (flat_ids[:, None] == jnp.arange(experts, dtype=jnp.int32)[None, :]).astype(jnp.int32)
    earlier = jnp.cumsum(matches, axis=0) - matches
    slot_index = jnp.sum(earlier * matches, axis=1)
    position = (
        flat_ids % local_count * (sources * capacity)
        + flat_ids // local_count * capacity
        + slot_index
    )
    buffer_rows = local_count * sources * capacity
    placed = (
        position.reshape(tok_rows, top_count)[:, :, None]
        == jnp.arange(buffer_rows, dtype=jnp.int32)[None, None, :]
    )
    placement_matrix = jnp.any(placed, axis=1).astype(jnp.bfloat16)
    outgoing = jnp.einsum("tp,td->pd", placement_matrix, normed, preferred_element_type=jnp.float32)
    outgoing = outgoing.astype(jnp.bfloat16).reshape(local_count, sources, capacity, columns)
    returned = jnp.concatenate(
        [
            expert_work(
                outgoing[number : number + 1],
                w_gate[number : number + 1],
                w_up[number : number + 1],
                w_down[number : number + 1],
            )
            for number in range(local_count)
        ],
        axis=0,
    )
    flat_out = returned.reshape(buffer_rows, columns)
    picked = flat_out[position].reshape(tok_rows, top_count, columns).astype(jnp.float32)
    return jnp.sum(picked * route_weights[:, :, None], axis=1).astype(jnp.bfloat16)


def solution(mesh):
    return jax.shard_map(
        per_device,
        mesh=mesh,
        in_specs=(
            P("ep", None),
            P(),
            P("ep", None),
            P("ep", None),
            P("ep", None, "tp"),
            P("ep", None, "tp"),
            P("ep", None, "tp"),
        ),
        out_specs=P("ep", "tp"),
        check_vma=False,
    )
```

profile of v0, /device:TPU:0, one launch (start us, length us, event | category | flops | bytes accessed | tf_op | source)
XLA Modules:
  0.0 269.5 jit_solution(14024327743090888040)
XLA Ops:
  6.5 0.9 copy.62
  7.4 0.1 eq.44
  7.6 0.1 eq.40
  7.7 4.5 %reduce-window.6 = s32[16,8,128]{2,1,0:T(8,128)S(1)} reduce-window(s32[16,8,128]{2,1,0:T(8,128)S(1)} %fusion.42, s32[]{:T(128)} %constant.28.clone.1), window={size=1x1x128 pad=0_0x0_0x127_0}, to_apply=%region_0.0 | reduce-window | flops 2080768 | bytes 131076 | tf_op jit(solution)/shard_map/reduce-window
  12.2 0.1 slice.50
  12.3 0.1 copy.64
  12.5 0.1 copy.65
  12.5 0.1 broadcast_add_fusion
  12.7 0.1 reduce_sum.41
  12.8 0.1 copy.66
  12.9 0.7 fusion.45
  13.6 1.7 fusion
  15.3 0.2 convert_reduce_fusion
  15.6 0.4 multiply_reduce_fusion.1
  16.0 0.8 dynamic_slice.7
  16.8 1.7 convolution_convert_fusion
  18.5 0.1 fusion.53
  18.6 27.2 %all_to_all.20 = bf16[1,8,96,512]{3,2,0,1:T(8,128)(2,1)} all-to-all(bf16[1,8,96,512]{3,2,0,1:T(8,128)(2,1)S(1)} %bitcast.82), channel_id=1, replica_groups=mesh['ep'=8,'tp'=4] {'ep'}, dimensions={1} | all-to-all | bytes 1572864 | tf_op jit(solution)/shard_map/all_to_all | solution.py:18
  45.8 0.0 all-gather.7.cloned.1.call-update
  45.8 0.0 all-gather.9.cloned.1.call-start
  45.9 24.0 %all_to_all.21 = bf16[1,8,96,512]{3,2,0,1:T(8,128)(2,1)} all-to-all(bf16[1,8,96,512]{3,2,0,1:T(8,128)(2,1)S(1)} %bitcast.81), channel_id=1, replica_groups=mesh['ep'=8,'tp'=4] {'ep'}, dimensions={1} | all-to-all | bytes 1572864 | tf_op jit(solution)/shard_map/all_to_all | solution.py:18
  69.9 0.0 all-gather.9.cloned.1.call-update
  69.9 0.0 all-gather.11.cloned.1.call-start
  70.0 18.6 %all-gather.7.cloned.1.call-done = bf16[1,768,2048]{2,1,0:T(8,128)(2,1)} async-done(((bf16[1,768,512]{2,1,0:T(8,128)(2,1)}), bf16[1,768,2048]{2,1,0:T(8,128)(2,1)}) %all-gather.7.cloned.1.call-update) | async-done | bytes 3145744 | tf_op jit(solution)/shard_map/all_gather | solution.py:22
  88.6 4.5 %fusion.7 = f32[768,512]{1,0:T(8,128)S(1)} fusion(bf16[1,768,2048]{2,1,0:T(8,128)(2,1)} %all-gather.7.cloned.1.call-done, bf16[2,2048,512]{2,1,0:T(8,128)(2,1)} %param.11), kind=kOutput, calls=%fused_computation.9 | convolution fusion | flops 1610612736 | bytes 6815744 | tf_op jit(solution)/shard_map/lrd,ldf->lrf/dot_general | solution.py:23
  93.1 0.2 copy-done.5
  93.3 3.0 %multiply_convert_fusion.1 = bf16[768,512]{1,0:T(8,128)(2,1)} fusion(f32[768,512]{1,0:T(8,128)S(1)} %fusion.7, bf16[2,2048,512]{2,1,0:T(8,128)(2,1)S(1)} %copy-done.2, bf16[1,768,2048]{2,1,0:T(8,128)(2,1)S(1)} %copy-done.5), kind=kOutput, calls=%fused_computation.32 | convolution fusion | flops 1614544896 | bytes 7602176 | tf_op jit(solution)/shard_map/lrd,ldf->lrf/dot_general | solution.py:26
  96.3 0.0 all-gather.11.cloned.1.call-update
  96.4 0.0 all-gather.13.cloned.1.call-start
  96.4 37.8 %all-gather.9.cloned.1.call-done = bf16[1,768,2048]{2,1,0:T(8,128)(2,1)} async-done(((bf16[1,768,512]{2,1,0:T(8,128)(2,1)}), bf16[1,768,2048]{2,1,0:T(8,128)(2,1)}) %all-gather.9.cloned.1.call-update) | async-done | bytes 3145744 | tf_op jit(solution)/shard_map/all_gather | solution.py:22
  134.2 4.5 %fusion.3 = f32[768,512]{1,0:T(8,128)S(1)} fusion(bf16[1,768,2048]{2,1,0:T(8,128)(2,1)} %all-gather.9.cloned.1.call-done, bf16[2,2048,512]{2,1,0:T(8,128)(2,1)} %param.11), kind=kOutput, calls=%fused_computation.5 | convolution fusion | flops 1610612736 | bytes 6815744 | tf_op jit(solution)/shard_map/lrd,ldf->lrf/dot_general | solution.py:23
  138.7 0.2 copy-done.4
  138.9 3.0 %multiply_convert_fusion = bf16[768,512]{1,0:T(8,128)(2,1)} fusion(f32[768,512]{1,0:T(8,128)S(1)} %fusion.3, bf16[2,2048,512]{2,1,0:T(8,128)(2,1)S(1)} %copy-done.3, bf16[1,768,2048]{2,1,0:T(8,128)(2,1)S(1)} %copy-done.4), kind=kOutput, calls=%fused_computation.31 | convolution fusion | flops 1614544896 | bytes 7602176 | tf_op jit(solution)/shard_map/lrd,ldf->lrf/dot_general | solution.py:26
  141.9 0.0 all-gather.13.cloned.1.call-update
  141.9 37.8 %all-gather.11.cloned.1.call-done = bf16[768,2048]{1,0:T(8,128)(2,1)} async-done(((bf16[768,512]{1,0:T(8,128)(2,1)}), bf16[768,2048]{1,0:T(8,128)(2,1)}) %all-gather.11.cloned.1.call-update) | async-done | bytes 3145744 | tf_op jit(solution)/shard_map/all_gather | solution.py:31
  179.8 5.2 %fusion.31 = bf16[768,512]{1,0:T(8,128)(2,1)} fusion(bf16[768,2048]{1,0:T(8,128)(2,1)} %all-gather.11.cloned.1.call-done, bf16[2,2048,512]{2,1,0:T(8,128)(2,1)} %param.13), kind=kOutput, calls=%fused_computation.33 | convolution fusion | flops 1611005952 | bytes 6029312 | tf_op jit(solution)/shard_map/lrf,lfd->lrd/dot_general | solution.py:29
  185.0 4.6 %all-to-all-start.1 = ((bf16[1,8,96,512]{3,2,0,1:T(8,128)(2,1)}), bf16[1,8,96,512]{3,2,0,1:T(8,128)(2,1)S(1)}, u32[]{:S(2)}, u32[]{:S(2)}) async-start(bf16[1,8,96,512]{3,2,0,1:T(8,128)(2,1)} %bitcast.10), calls=%async_computation.1 | async-start | bytes 1572864 | tf_op jit(solution)/shard_map/all_to_all | solution.py:36
  189.6 35.6 %all-gather.13.cloned.1.call-done = bf16[768,2048]{1,0:T(8,128)(2,1)} async-done(((bf16[768,512]{1,0:T(8,128)(2,1)}), bf16[768,2048]{1,0:T(8,128)(2,1)}) %all-gather.13.cloned.1.call-update) | async-done | bytes 3145744 | tf_op jit(solution)/shard_map/all_gather | solution.py:31
  225.2 5.2 %fusion.34 = bf16[768,512]{1,0:T(8,128)(2,1)} fusion(bf16[768,2048]{1,0:T(8,128)(2,1)} %all-gather.13.cloned.1.call-done, bf16[2,2048,512]{2,1,0:T(8,128)(2,1)} %param.13), kind=kOutput, calls=%fused_computation.34 | convolution fusion | flops 1611005952 | bytes 6029312 | tf_op jit(solution)/shard_map/lrf,lfd->lrd/dot_general | solution.py:29
  230.4 4.6 %all-to-all-start.3 = ((bf16[1,8,96,512]{3,2,0,1:T(8,128)(2,1)}), bf16[1,8,96,512]{3,2,0,1:T(8,128)(2,1)S(1)}, u32[]{:S(2)}, u32[]{:S(2)}) async-start(bf16[1,8,96,512]{3,2,0,1:T(8,128)(2,1)} %bitcast.19), calls=%async_computation.3 | async-start | bytes 1572864 | tf_op jit(solution)/shard_map/all_to_all | solution.py:36
  235.0 0.1 reshape.289
  235.1 0.1 copy.73
  235.3 20.6 %all-to-all-done.3 = bf16[1,8,96,512]{3,2,0,1:T(8,128)(2,1)S(1)} async-done(((bf16[1,8,96,512]{3,2,0,1:T(8,128)(2,1)}), bf16[1,8,96,512]{3,2,0,1:T(8,128)(2,1)S(1)}, u32[]{:S(2)}, u32[]{:S(2)}) %all-to-all-start.3) | async-done | bytes 786464 | tf_op jit(solution)/shard_map/all_to_all | solution.py:36
  255.9 0.1 pad_maximum_fusion
  256.1 0.1 copy.71
  256.2 4.0 %gather_fusion = bf16[1024,512]{1,0:T(8,128)(2,1)S(1)} fusion(bf16[1536,512]{1,0:T(8,128)(2,1)S(1)} %bitcast.78, s32[1024]{0:T(1024)S(1)} %broadcast_clamp_fusion), kind=kCustom, calls=%fused_computation | custom fusion | bytes 2101248 | tf_op jit(solution)/shard_map/gather | solution.py:86
  260.2 0.7 reshape.290
  260.9 2.1 multiply_reduce_fusion
  (20 shorter events, 0.2 us)
Async XLA Ops:
  6.5 8.8 %copy-start = (bf16[256,2048]{1,0:T(8,128)(2,1)S(1)}, bf16[256,2048]{1,0:T(8,128)(2,1)}, u32[]{:S(2)}) copy-start(bf16[256,2048]{1,0:T(8,128)(2,1)} %param.7) | copy-start | bytes 3145732
  6.5 82.1 %all-gather.7.cloned.1.call-start = ((), (), s32[]{:S(2)}) async-start(), calls=%async_computation.4 | async-start | bytes 3932160 | tf_op jit(solution)/shard_map/all_gather | solution.py:22
  45.8 88.4 %all-gather.9.cloned.1.call-start = ((), (), s32[]{:S(2)}) async-start(), calls=%async_computation.5 | async-start | bytes 3932160 | tf_op jit(solution)/shard_map/all_gather | solution.py:22
  69.9 109.8 %all-gather.11.cloned.1.call-start = ((), (), s32[]{:S(2)}) async-start(), calls=%async_computation.6 | async-start | bytes 3932160 | tf_op jit(solution)/shard_map/all_gather | solution.py:31
  88.6 4.5 %copy-start.2 = (bf16[2,2048,512]{2,1,0:T(8,128)(2,1)S(1)}, bf16[2,2048,512]{2,1,0:T(8,128)(2,1)}, u32[]{:S(2)}) copy-start(bf16[2,2048,512]{2,1,0:T(8,128)(2,1)} %param.12) | copy-start | bytes 12582916
  88.6 4.7 %copy-start.5 = (bf16[1,768,2048]{2,1,0:T(8,128)(2,1)S(1)}, bf16[1,768,2048]{2,1,0:T(8,128)(2,1)}, u32[]{:S(2)}) copy-start(bf16[1,768,2048]{2,1,0:T(8,128)(2,1)} %all-gather.7.cloned.1.call-done) | copy-start | bytes 9437188
  96.4 128.8 %all-gather.13.cloned.1.call-start = ((), (), s32[]{:S(2)}) async-start(), calls=%async_computation.7 | async-start | bytes 3932160 | tf_op jit(solution)/shard_map/all_gather | solution.py:31
  134.2 4.5 %copy-start.3 = (bf16[2,2048,512]{2,1,0:T(8,128)(2,1)S(1)}, bf16[2,2048,512]{2,1,0:T(8,128)(2,1)}, u32[]{:S(2)}) copy-start(bf16[2,2048,512]{2,1,0:T(8,128)(2,1)} %param.12) | copy-start | bytes 12582916
  134.2 4.7 %copy-start.4 = (bf16[1,768,2048]{2,1,0:T(8,128)(2,1)S(1)}, bf16[1,768,2048]{2,1,0:T(8,128)(2,1)}, u32[]{:S(2)}) copy-start(bf16[1,768,2048]{2,1,0:T(8,128)(2,1)} %all-gather.9.cloned.1.call-done) | copy-start | bytes 9437188
  185.0 45.4 %all-to-all-start.1 = ((bf16[1,8,96,512]{3,2,0,1:T(8,128)(2,1)}), bf16[1,8,96,512]{3,2,0,1:T(8,128)(2,1)S(1)}, u32[]{:S(2)}, u32[]{:S(2)}) async-start(bf16[1,8,96,512]{3,2,0,1:T(8,128)(2,1)} %bitcast.10), calls=%async_computation.1 | async-start | bytes 1572864 | tf_op jit(solution)/shard_map/all_to_all | solution.py:36
  189.6 45.5 %copy-start.1 = (f32[256,4]{0,1:T(4,128)S(1)}, f32[256,4]{0,1:T(4,128)}, u32[]{:S(2)}) copy-start(f32[256,4]{0,1:T(4,128)} %param.10) | copy-start | bytes 12292
  230.4 25.6 %all-to-all-start.3 = ((bf16[1,8,96,512]{3,2,0,1:T(8,128)(2,1)}), bf16[1,8,96,512]{3,2,0,1:T(8,128)(2,1)S(1)}, u32[]{:S(2)}, u32[]{:S(2)}) async-start(bf16[1,8,96,512]{3,2,0,1:T(8,128)(2,1)} %bitcast.19), calls=%async_computation.3 | async-start | bytes 1572864 | tf_op jit(solution)/shard_map/all_to_all | solution.py:36
Sparse Core Ops, SparseCore 0:
  45.9 42.6 all-gather.6
  90.4 43.6 all-gather.8
  136.0 43.6 all-gather.10
  181.4 43.6 all-gather.12
where the time goes:
time: 270 us; the launch traced here: 269 us
  waiting for transfers between devices  150 us (56%)
  blocking collectives  51.2 us (19%)
  matrix products  27 us (10%)
  between operations  13.3 us (5%)
  other arithmetic  10 us (4%)
  starting transfers between devices  9.36 us (3%)
  local copies, waits for them, and re-layouts  8.03 us (3%)
    all_gather x2, waiting for transfers between devices, expert_work(): lax.all_gather(activation, 'tp', axis=2, tiled=True)  73.4 us
    all_gather x2, waiting for transfers between devices, expert_work(): shard_piece = lax.all_gather(row_block, 'tp', axis=2, tiled=True)  56.4 us
    all_to_all x2, blocking collectives, expert_work(): lax.all_to_all(outgoing, 'ep', split_axis=1, concat_axis=1, tiled=True)  51.2 us
    all_to_all x2, waiting for transfers between devices, expert_work(): return lax.all_to_all(result, 'ep', split_axis=1, concat_axis=1, tiled=True)  20.6 us
    dot_general x2, matrix products, expert_work(): jnp.einsum('lrf,lfd->lrd', lax.all_gather(activation, 'tp', axis=2, tiled...  10.4 us
    all_to_all x2, starting transfers between devices, expert_work(): return lax.all_to_all(result, 'ep', split_axis=1, concat_axis=1, tiled=True)  9.23 us
    dot_general x2, matrix products, expert_work(): jnp.einsum('lrd,ldf->lrf', shard_piece, gate_weight, preferred_element_ty...  8.95 us
    dot_general x2, matrix products, expert_work(): jnp.einsum('lrd,ldf->lrf', shard_piece, up_weight, preferred_element_type...  5.99 us
  transfers between devices with their start and end apart: 6, of which 5 were waited for; matrix products, arithmetic and copies ran while one was open for 10% of the time, Pallas kernels for 0%

commit v1 on v0

--- a/solution.py
+++ b/solution.py
@@ -6,6 +6,22 @@
 swiglu_limit = 7.0
 swiglu_alpha = 1.702
 norm_eps = 1e-05
+
+
+def ring_product(x, axis, dim, term):
+    length, index, rows = (lax.axis_size(axis), lax.axis_index(axis), x.shape[dim])
+    right = [(i, (i + 1) % length) for i in range(length)]
+    left = [(i, (i - 1) % length) for i in range(length)]
+    middle = length // 2
+    from_left = from_right = x
+    total = term(x, index * rows)
+    for step in range(1, middle + 1):
+        from_left = lax.ppermute(from_left, axis, right)
+        if step < length - middle:
+            from_right = lax.ppermute(from_right, axis, left)
+            total = total + term(from_right, (index + step) % length * rows)
+        total = total + term(from_left, (index - step) % length * rows)
+    return total
 
 
 def clamped_units(gate_pre, up_pre):
@@ -26,11 +42,16 @@
     up_sum = jnp.einsum("lrd,ldf->lrf", shard_piece, up_weight, preferred_element_type=jnp.float32)
     activation = clamped_units(gate_sum, up_sum).astype(jnp.bfloat16)
     out_cols = down_weight.shape[2]
-    result = jnp.einsum(
-        "lrf,lfd->lrd",
-        lax.all_gather(activation, "tp", axis=2, tiled=True),
-        down_weight,
-        preferred_element_type=jnp.float32,
+    result = ring_product(
+        activation,
+        "tp",
+        2,
+        lambda shard, at: jnp.einsum(
+            "lrf,lfd->lrd",
+            shard,
+            lax.dynamic_slice_in_dim(down_weight, at, shard.shape[2], axis=1),
+            preferred_element_type=jnp.float32,
+        ),
     )
     result = result.astype(jnp.bfloat16).reshape(local_count, sources, capacity, out_cols)
     return lax.all_to_all(result, "ep", split_axis=1, concat_axis=1, tiled=True)

time: 270 us -> 288 us (1.067)
  starting transfers between devices: 9.36 us -> 17.6 us
  waiting for transfers between devices: 150 us -> 155 us
  local copies, waits for them, and re-layouts: 8.03 us -> 12.1 us
    all_gather x2 -> x0, waiting for transfers between devices: 73.4 us -> none  [expert_work(): lax.all_gather(activation, 'tp', axis=2, tiled=True)]
    ppermute x0 -> x6, waiting for transfers between devices: none -> 60.1 us  [the longest x4 60.1 us: ring_product(): from_left = lax.ppermute(from_left, axis, right)]
    all_gather x2, waiting for transfers between devices: 56.4 us -> 74.1 us  [expert_work(): shard_piece = lax.all_gather(row_block, 'tp', axis=2, tiled=True)]
    ppermute x0 -> x6, starting transfers between devices: none -> 8.14 us  [the longest x4 5.2 us: ring_product(): from_left = lax.ppermute(from_left, axis, right)]
    slice x2 -> x3, local copies, waits for them, and re-layouts: 0.21 us -> 4.23 us  [the longest x1 4.03 us: per_device(): w_down[number:number + 1]]
    dot_general x2 -> x8, matrix products: 10.4 us -> 12.1 us  [expert_work(): jnp.einsum('lrf,lfd->lrd', shard, lax.dynamic_slice_in_dim(down_weight, a...]
  transfers between devices with their start and end apart: 6 -> 10, of which waited for: 5 -> 5; matrix products, arithmetic and copies ran while one was open for 10% -> 11% of each run, Pallas kernels for 0% -> 0%
where the time goes in v1:
time: 288 us; the launch traced here: 287 us
  waiting for transfers between devices  155 us (54%)
  blocking collectives  51.2 us (18%)
  matrix products  27.9 us (10%)
  starting transfers between devices  17.6 us (6%)
  between operations  13.7 us (5%)
  local copies, waits for them, and re-layouts  12.1 us (4%)
  other arithmetic  10 us (3%)
    all_gather x2, waiting for transfers between devices, expert_work(): shard_piece = lax.all_gather(row_block, 'tp', axis=2, tiled=True)  74.1 us
    ppermute x4, waiting for transfers between devices, ring_product(): from_left = lax.ppermute(from_left, axis, right)  60.1 us
    all_to_all x2, blocking collectives, expert_work(): lax.all_to_all(outgoing, 'ep', split_axis=1, concat_axis=1, tiled=True)  51.2 us
    all_to_all x2, waiting for transfers between devices, expert_work(): return lax.all_to_all(result, 'ep', split_axis=1, concat_axis=1, tiled=True)  20.6 us
    dot_general x8, matrix products, expert_work(): jnp.einsum('lrf,lfd->lrd', shard, lax.dynamic_slice_in_dim(down_weight, a...  12.1 us
    all_to_all x2, starting transfers between devices, expert_work(): return lax.all_to_all(result, 'ep', split_axis=1, concat_axis=1, tiled=True)  9.45 us
    dot_general x2, matrix products, expert_work(): jnp.einsum('lrd,ldf->lrf', shard_piece, gate_weight, preferred_element_ty...  8.93 us
  transfers between devices with their start and end apart: 10, of which 5 were waited for; matrix products, arithmetic and copies ran while one was open for 11% of the time, Pallas kernels for 0%

profile of v1, /device:TPU:0, one launch (start us, length us, event | category | flops | bytes accessed | tf_op | source)
XLA Modules:
  0.0 287.3 jit_solution(413537357020292983)
XLA Ops:
  6.5 0.9 copy.62
  7.4 0.1 eq.51
  7.6 0.1 eq.47
  7.7 4.5 %reduce-window.6 = s32[16,8,128]{2,1,0:T(8,128)S(1)} reduce-window(s32[16,8,128]{2,1,0:T(8,128)S(1)} %fusion.58, s32[]{:T(128)} %constant.76.clone.1), window={size=1x1x128 pad=0_0x0_0x127_0}, to_apply=%region_0.0 | reduce-window | flops 2080768 | bytes 131076 | tf_op jit(solution)/shard_map/reduce-window
  12.3 0.1 copy.64
  12.7 0.1 reduce_sum.41
  12.9 0.7 fusion.61
  13.6 1.7 fusion
  15.3 0.2 convert_reduce_fusion
  15.6 0.4 multiply_reduce_fusion.1
  16.0 0.8 dynamic_slice.31
  16.8 1.7 convolution_convert_fusion
  18.6 27.2 %all_to_all.20 = bf16[1,8,96,512]{3,2,0,1:T(8,128)(2,1)} all-to-all(bf16[1,8,96,512]{3,2,0,1:T(8,128)(2,1)S(1)} %bitcast.116), channel_id=1, replica_groups=mesh['ep'=8,'tp'=4] {'ep'}, dimensions={1} | all-to-all | bytes 1572864 | tf_op jit(solution)/shard_map/all_to_all | solution.py:34
  45.8 24.0 %all_to_all.21 = bf16[1,8,96,512]{3,2,0,1:T(8,128)(2,1)} all-to-all(bf16[1,8,96,512]{3,2,0,1:T(8,128)(2,1)S(1)} %bitcast.115), channel_id=1, replica_groups=mesh['ep'=8,'tp'=4] {'ep'}, dimensions={1} | all-to-all | bytes 1572864 | tf_op jit(solution)/shard_map/all_to_all | solution.py:34
  70.0 4.0 %fusion.77 = (bf16[1,2048,512]{2,1,0:T(8,128)(2,1)}, bf16[1,2048,512]{2,1,0:T(8,128)(2,1)S(1)}) fusion(bf16[2,2048,512]{2,1,0:T(8,128)(2,1)} %param.13), kind=kLoop, calls=%fused_computation.101 | loop fusion | bytes 8388608 | tf_op jit(solution)/shard_map/slice | solution.py:100
  74.0 14.6 %all-gather.3.cloned.1.call-done = bf16[1,768,2048]{2,1,0:T(8,128)(2,1)} async-done(((bf16[1,768,512]{2,1,0:T(8,128)(2,1)}), bf16[1,768,2048]{2,1,0:T(8,128)(2,1)}) %all-gather.3.cloned.1.call-update) | async-done | bytes 3145744 | tf_op jit(solution)/shard_map/all_gather | solution.py:38
  88.6 4.5 %fusion.7 = f32[768,512]{1,0:T(8,128)S(1)} fusion(bf16[1,768,2048]{2,1,0:T(8,128)(2,1)} %all-gather.3.cloned.1.call-done, bf16[2,2048,512]{2,1,0:T(8,128)(2,1)} %param.11), kind=kOutput, calls=%fused_computation.9 | convolution fusion | flops 1610612736 | bytes 6815744 | tf_op jit(solution)/shard_map/lrd,ldf->lrf/dot_general | solution.py:39
  93.1 0.3 copy-done.6
  93.3 2.1 multiply_convert_fusion.1
  95.5 1.5 collective-permute-start.1
  97.0 1.5 collective-permute-start
  98.4 59.5 %all-gather.5.cloned.1.call-done = bf16[1,768,2048]{2,1,0:T(8,128)(2,1)} async-done(((bf16[1,768,512]{2,1,0:T(8,128)(2,1)}), bf16[1,768,2048]{2,1,0:T(8,128)(2,1)}) %all-gather.5.cloned.1.call-update) | async-done | bytes 3145744 | tf_op jit(solution)/shard_map/all_gather | solution.py:38
  157.9 4.5 %fusion.3 = f32[768,512]{1,0:T(8,128)S(1)} fusion(bf16[1,768,2048]{2,1,0:T(8,128)(2,1)} %all-gather.5.cloned.1.call-done, bf16[2,2048,512]{2,1,0:T(8,128)(2,1)} %param.11), kind=kOutput, calls=%fused_computation.5 | convolution fusion | flops 1610612736 | bytes 6815744 | tf_op jit(solution)/shard_map/lrd,ldf->lrf/dot_general | solution.py:39
  162.4 0.3 copy-done.5
  162.6 3.0 %multiply_convert_fusion = bf16[768,512]{1,0:T(8,128)(2,1)} fusion(f32[768,512]{1,0:T(8,128)S(1)} %fusion.3, bf16[2,2048,512]{2,1,0:T(8,128)(2,1)S(1)} %copy-done.4, bf16[1,768,2048]{2,1,0:T(8,128)(2,1)S(1)} %copy-done.5), kind=kOutput, calls=%fused_computation.26 | convolution fusion | flops 1614544896 | bytes 7602176 | tf_op jit(solution)/shard_map/lrd,ldf->lrf/dot_general | solution.py:42
  165.6 1.5 collective-permute-start.3
  167.1 0.5 collective-permute-start.4
  167.7 1.5 collective-permute-start.2
  169.2 0.6 fusion.43
  169.7 1.7 fusion.31
  171.4 1.7 fusion.33
  173.2 45.8 %collective-permute-done.2 = bf16[1,768,512]{2,1,0:T(8,128)(2,1)S(1)} collective-permute-done((bf16[1,768,512]{2,1,0:T(8,128)(2,1)}, bf16[1,768,512]{2,1,0:T(8,128)(2,1)S(1)}, u32[]{:S(2)}, u32[]{:S(2)}) %collective-permute-start.2) | collective-permute-done | bytes 786464 | tf_op jit(solution)/shard_map/ppermute | solution.py:19
  218.9 1.6 add_convert_fusion.1
  220.5 4.6 %all-to-all-start.1 = ((bf16[1,8,96,512]{3,2,0,1:T(8,128)(2,1)}), bf16[1,8,96,512]{3,2,0,1:T(8,128)(2,1)S(1)}, u32[]{:S(2)}, u32[]{:S(2)}) async-start(bf16[1,8,96,512]{3,2,0,1:T(8,128)(2,1)} %bitcast.117), calls=%async_computation.1 | async-start | bytes 1572864 | tf_op jit(solution)/shard_map/all_to_all | solution.py:57
  225.1 1.6 collective-permute-start.5
  226.8 1.7 fusion.38
  228.5 1.7 fusion.26
  230.2 1.7 fusion.28
  231.9 14.3 %collective-permute-done.5 = bf16[1,768,512]{2,1,0:T(8,128)(2,1)S(1)} collective-permute-done((bf16[1,768,512]{2,1,0:T(8,128)(2,1)}, bf16[1,768,512]{2,1,0:T(8,128)(2,1)S(1)}, u32[]{:S(2)}, u32[]{:S(2)}) %collective-permute-start.5) | collective-permute-done | bytes 786464 | tf_op jit(solution)/shard_map/ppermute | solution.py:19
  246.2 1.5 add_convert_fusion
  247.7 4.8 %all-to-all-start.3 = ((bf16[1,8,96,512]{3,2,0,1:T(8,128)(2,1)}), bf16[1,8,96,512]{3,2,0,1:T(8,128)(2,1)S(1)}, u32[]{:S(2)}, u32[]{:S(2)}) async-start(bf16[1,8,96,512]{3,2,0,1:T(8,128)(2,1)} %bitcast.118), calls=%async_computation.3 | async-start | bytes 1572864 | tf_op jit(solution)/shard_map/all_to_all | solution.py:57
  252.5 0.1 reshape.345
  252.7 0.1 copy.73
  252.9 20.6 %all-to-all-done.3 = bf16[1,8,96,512]{3,2,0,1:T(8,128)(2,1)S(1)} async-done(((bf16[1,8,96,512]{3,2,0,1:T(8,128)(2,1)}), bf16[1,8,96,512]{3,2,0,1:T(8,128)(2,1)S(1)}, u32[]{:S(2)}, u32[]{:S(2)}) %all-to-all-start.3) | async-done | bytes 786464 | tf_op jit(solution)/shard_map/all_to_all | solution.py:57
  273.5 0.1 pad_maximum_fusion
  273.7 4.0 %gather_fusion = bf16[1024,512]{1,0:T(8,128)(2,1)S(1)} fusion(bf16[1536,512]{1,0:T(8,128)(2,1)S(1)} %bitcast.112, s32[1024]{0:T(1024)S(1)} %broadcast_clamp_fusion), kind=kCustom, calls=%fused_computation | custom fusion | bytes 2101248 | tf_op jit(solution)/shard_map/gather | solution.py:107
  277.7 0.7 reshape.346
  278.4 2.1 multiply_reduce_fusion
  (35 shorter events, 0.8 us)
Async XLA Ops:
  6.5 8.8 %copy-start.1 = (bf16[256,2048]{1,0:T(8,128)(2,1)S(1)}, bf16[256,2048]{1,0:T(8,128)(2,1)}, u32[]{:S(2)}) copy-start(bf16[256,2048]{1,0:T(8,128)(2,1)} %param.7) | copy-start | bytes 3145732
  6.5 82.1 %all-gather.3.cloned.1.call-start = ((), (), s32[]{:S(2)}) async-start(), calls=%async_computation.4 | async-start | bytes 3932160 | tf_op jit(solution)/shard_map/all_gather | solution.py:38
  45.8 112.1 %all-gather.5.cloned.1.call-start = ((), (), s32[]{:S(2)}) async-start(), calls=%async_computation.5 | async-start | bytes 3932160 | tf_op jit(solution)/shard_map/all_gather | solution.py:38
  88.6 4.5 %copy-start.3 = (bf16[2,2048,512]{2,1,0:T(8,128)(2,1)S(1)}, bf16[2,2048,512]{2,1,0:T(8,128)(2,1)}, u32[]{:S(2)}) copy-start(bf16[2,2048,512]{2,1,0:T(8,128)(2,1)} %param.12) | copy-start | bytes 12582916
  88.6 4.7 %copy-start.6 = (bf16[1,768,2048]{2,1,0:T(8,128)(2,1)S(1)}, bf16[1,768,2048]{2,1,0:T(8,128)(2,1)}, u32[]{:S(2)}) copy-start(bf16[1,768,2048]{2,1,0:T(8,128)(2,1)} %all-gather.3.cloned.1.call-done) | copy-start | bytes 9437188
  95.5 72.2 %collective-permute-start.1 = (bf16[1,768,512]{2,1,0:T(8,128)(2,1)S(1)}, bf16[1,768,512]{2,1,0:T(8,128)(2,1)}, u32[]{:S(2)}, u32[]{:S(2)}) collective-permute-start(bf16[1,768,512]{2,1,0:T(8,128)(2,1)S(1)} %bitcast.119), channel_id=1, source_target_pairs={{0,1},{1,2},{2,3},{3,0},{4,5},{5,6},{6,7},{7,4},{8,9},{9,10},{10,1... | collective-permute-start | bytes 2359304 | tf_op jit(solution)/shard_map/ppermute | solution.py:19
  97.0 74.5 %collective-permute-start = (bf16[1,768,512]{2,1,0:T(8,128)(2,1)S(1)}, bf16[1,768,512]{2,1,0:T(8,128)(2,1)}, u32[]{:S(2)}, u32[]{:S(2)}) collective-permute-start(bf16[1,768,512]{2,1,0:T(8,128)(2,1)S(1)} %bitcast.120), channel_id=1, source_target_pairs={{0,3},{1,0},{2,1},{3,2},{4,7},{5,4},{6,5},{7,6},{8,11},{9,8},{10,9... | collective-permute-start | bytes 2359304 | tf_op jit(solution)/shard_map/ppermute | solution.py:21
  157.9 4.5 %copy-start.4 = (bf16[2,2048,512]{2,1,0:T(8,128)(2,1)S(1)}, bf16[2,2048,512]{2,1,0:T(8,128)(2,1)}, u32[]{:S(2)}) copy-start(bf16[2,2048,512]{2,1,0:T(8,128)(2,1)} %param.12) | copy-start | bytes 12582916
  157.9 4.7 %copy-start.5 = (bf16[1,768,2048]{2,1,0:T(8,128)(2,1)S(1)}, bf16[1,768,2048]{2,1,0:T(8,128)(2,1)}, u32[]{:S(2)}) copy-start(bf16[1,768,2048]{2,1,0:T(8,128)(2,1)} %all-gather.5.cloned.1.call-done) | copy-start | bytes 9437188
  162.6 6.5 %copy-start = (bf16[1,2048,512]{2,1,0:T(8,128)(2,1)S(1)}, bf16[1,2048,512]{2,1,0:T(8,128)(2,1)}, u32[]{:S(2)}) copy-start(bf16[1,2048,512]{2,1,0:T(8,128)(2,1)} %get-tuple-element.5) | copy-start | bytes 6291460
  165.6 64.6 %collective-permute-start.3 = (bf16[1,768,512]{2,1,0:T(8,128)(2,1)}, bf16[1,768,512]{2,1,0:T(8,128)(2,1)}, u32[]{:S(2)}, u32[]{:S(2)}) collective-permute-start(bf16[1,768,512]{2,1,0:T(8,128)(2,1)} %bitcast.25), channel_id=1, source_target_pairs={{0,3},{1,0},{2,1},{3,2},{4,7},{5,4},{6,5},{7,6},{8,11},{9,8},{10,9... | collective-permute-start | bytes 2359304 | tf_op jit(solution)/shard_map/ppermute | solution.py:21
  167.1 58.0 %collective-permute-start.4 = (bf16[1,768,512]{2,1,0:T(8,128)(2,1)}, bf16[1,768,512]{2,1,0:T(8,128)(2,1)}, u32[]{:S(2)}, u32[]{:S(2)}) collective-permute-start(bf16[1,768,512]{2,1,0:T(8,128)(2,1)} %bitcast.25), channel_id=1, source_target_pairs={{0,1},{1,2},{2,3},{3,0},{4,5},{5,6},{6,7},{7,4},{8,9},{9,10},{10,1... | collective-permute-start | bytes 2359304 | tf_op jit(solution)/shard_map/ppermute | solution.py:19
  167.7 51.3 %collective-permute-start.2 = (bf16[1,768,512]{2,1,0:T(8,128)(2,1)}, bf16[1,768,512]{2,1,0:T(8,128)(2,1)S(1)}, u32[]{:S(2)}, u32[]{:S(2)}) collective-permute-start(bf16[1,768,512]{2,1,0:T(8,128)(2,1)} %collective-permute-done.1), channel_id=1, source_target_pairs={{0,1},{1,2},{2,3},{3,0},{4,5},{5,6},{6,7},{7,4},{8,9},{9,10},{10,1... | collective-permute-start | bytes 2359304 | tf_op jit(solution)/shard_map/ppermute | solution.py:19
  220.5 27.2 %all-to-all-start.1 = ((bf16[1,8,96,512]{3,2,0,1:T(8,128)(2,1)}), bf16[1,8,96,512]{3,2,0,1:T(8,128)(2,1)S(1)}, u32[]{:S(2)}, u32[]{:S(2)}) async-start(bf16[1,8,96,512]{3,2,0,1:T(8,128)(2,1)} %bitcast.117), calls=%async_computation.1 | async-start | bytes 1572864 | tf_op jit(solution)/shard_map/all_to_all | solution.py:57
  225.1 21.1 %collective-permute-start.5 = (bf16[1,768,512]{2,1,0:T(8,128)(2,1)}, bf16[1,768,512]{2,1,0:T(8,128)(2,1)S(1)}, u32[]{:S(2)}, u32[]{:S(2)}) collective-permute-start(bf16[1,768,512]{2,1,0:T(8,128)(2,1)} %collective-permute-done.4), channel_id=1, source_target_pairs={{0,1},{1,2},{2,3},{3,0},{4,5},{5,6},{6,7},{7,4},{8,9},{9,10},{10,1... | collective-permute-start | bytes 2359304 | tf_op jit(solution)/shard_map/ppermute | solution.py:19
  247.7 5.0 %copy-start.2 = (f32[256,4]{0,1:T(4,128)S(1)}, f32[256,4]{0,1:T(4,128)}, u32[]{:S(2)}) copy-start(f32[256,4]{0,1:T(4,128)} %param.10) | copy-start | bytes 12292
  247.7 25.8 %all-to-all-start.3 = ((bf16[1,8,96,512]{3,2,0,1:T(8,128)(2,1)}), bf16[1,8,96,512]{3,2,0,1:T(8,128)(2,1)S(1)}, u32[]{:S(2)}, u32[]{:S(2)}) async-start(bf16[1,8,96,512]{3,2,0,1:T(8,128)(2,1)} %bitcast.118), calls=%async_computation.3 | async-start | bytes 1572864 | tf_op jit(solution)/shard_map/all_to_all | solution.py:57
Sparse Core Ops, SparseCore 0:
  45.9 42.6 all-gather.2
  90.4 67.4 all-gather.4
